TPU v7x, 512 devices: a whole 4x4x16 slice. The times are simulated.
512 devices in a mesh: rep: 2 (over z_hi), fs: 32 (over z_lo, y), tp: 8 (over x, core).
Axes of the slice: x: 4, y: 4, z: 16 (z_hi: 2, z_lo: 8; z = z_hi * 8 + z_lo), core: 2. Of those that a mesh axis runs over, the one named last changes fastest.
Arguments:
- stream: bfloat16 [16384, 2048], P(('rep', 'fs'), 'tp'), may hold values from -6 to 6
- norm_gains: float32 [6, 2048], replicated, may hold values from 0.1 to 1.9
- w_gate: bfloat16 [2048, 5632], P('fs', 'tp'), may hold values from -0.125 to 0.125
- w_up: bfloat16 [2048, 5632], P('fs', 'tp'), may hold values from -0.125 to 0.125
- w_down: bfloat16 [5632, 2048], P('tp', 'fs'), may hold values from -0.15625 to 0.15625
- w_inner: bfloat16 [2048, 1024], P('fs', 'tp'), may hold values from -0.125 to 0.125
- w_bgate: bfloat16 [2048, 1024], P('fs', 'tp'), may hold values from -0.125 to 0.125
- w_cgate: bfloat16 [2048, 1024], P('fs', 'tp'), may hold values from -0.125 to 0.125
- conv_taps: float32 [3, 1024], P(None, 'tp'), may hold values from -3.5 to 3.5
- w_out: bfloat16 [1024, 2048], P('tp', 'fs'), may hold values from -0.375 to 0.375
Outputs:
- mixed: bfloat16 [16384, 2048], P(('rep', 'fs'), 'tp')
All inputs are finite; a program needn't handle non-finite values.
Results may differ from a plain program's by a relative error of at most 0.02.
Values may be sent and summed in bfloat16 or wider, within the bound.
A program may use at most 64 MiB of HBM per device.

v0:
```python
import jax
import jax.numpy as jnp
from jax import lax
from jax.sharding import PartitionSpec as P

TAPS = 3
EPSILON = 1e-06


def laid_out(parts, dim):
    shape = list(parts.shape[1:])
    shape[dim] *= parts.shape[0]
    return jnp.moveaxis(parts, 0, dim).reshape(shape)


def from_everyone(x, axis):
    copies = jnp.broadcast_to(x, (lax.axis_size(axis), *x.shape))
    return lax.all_to_all(copies, axis, split_axis=0, concat_axis=0, tiled=True)


def collect(x, axis, dim):
    return laid_out(from_everyone(x, axis), dim)


def cut_along(x, dim, count):
    shape = x.shape
    parts = x.reshape(*shape[:dim], count, shape[dim] // count, *shape[dim + 1 :])
    return jnp.moveaxis(parts, dim, 0)


def sent_and_summed(x, axis, dim):
    parts = cut_along(x, dim, lax.axis_size(axis))
    arrived = lax.all_to_all(parts, axis, split_axis=0, concat_axis=0, tiled=True)
    return arrived.astype(jnp.float32).sum(axis=0)


def taken_together(x, axis):
    everything = from_everyone(x, axis)
    return jnp.sum(everything, axis=0)


def rows_first(arrays, axis, dims):
    turned = [jnp.moveaxis(a, dim, 0) for a, dim in zip(arrays, dims)]
    both = jnp.concatenate([t.reshape(len(t), -1) for t in turned], axis=1)
    whole, at, done = (lax.all_gather(both, axis, axis=0, tiled=True), 0, [])
    for t, dim in zip(turned, dims):
        slab = whole[:, at : at + t[0].size].reshape(-1, *t.shape[1:])
        done.append(jnp.moveaxis(slab, 0, dim))
        at += t[0].size
    return tuple(done)


def from_behind(x, axis, by):
    count = lax.axis_size(axis)
    pairs = [(i, i + by) for i in range(count) if 0 <= i + by < count]
    return lax.ppermute(x, axis, pairs)


def shards(stream, norm_gains, w_gate, w_up, w_down, w_inner, w_bgate, w_cgate, conv_taps, w_out):
    tp_index = lax.axis_index("tp")
    local_width = stream.shape[1]
    model_width = local_width * lax.axis_size("tp")

    def own_gain(row):
        return lax.dynamic_slice_in_dim(norm_gains[row], tp_index * local_width, local_width, 0)

    def gathered_norm(current, row):
        gathered = collect(current, "tp", 1)
        values = gathered.astype(jnp.float32)
        scaled = values * lax.rsqrt(jnp.mean(values * values, axis=1, keepdims=True) + EPSILON)
        return (scaled * norm_gains[row]).astype(jnp.bfloat16)

    def settle(current, partials, row, weight):
        branch_sum = sent_and_summed(partials.astype(jnp.bfloat16), "tp", 1)
        squares = taken_together(jnp.sum(branch_sum * branch_sum, axis=1), "tp")
        scaled = branch_sum * lax.rsqrt(squares / model_width + EPSILON)[:, None]
        return (current.astype(jnp.float32) + weight * (scaled * own_gain(row))).astype(
            jnp.bfloat16
        )

    gate_whole, up_whole, down_whole = rows_first((w_gate, w_up, w_down), "fs", (0, 0, 1))

    def feed_forward(current, row_in, row_out):
        normed = gathered_norm(current, row_in)
        gate_vals = jnp.dot(normed, gate_whole, preferred_element_type=jnp.float32)
        upward = jnp.dot(normed, up_whole, preferred_element_type=jnp.float32)
        hidden = (jax.nn.silu(gate_vals) * upward).astype(jnp.bfloat16)
        partials = jnp.dot(hidden, down_whole, preferred_element_type=jnp.float32)
        return settle(current, partials, row_out, 0.5)

    first = feed_forward(stream, 0, 1)
    normed_mix = gathered_norm(first, 2)
    local_rows = normed_mix.shape[0]

    def fold_rows(block_rows):
        return jnp.dot(normed_mix, block_rows, preferred_element_type=jnp.float32)

    inner = fold_rows(collect(w_inner, "fs", 0))
    bgate = fold_rows(collect(w_bgate, "fs", 0))
    cgate = fold_rows(collect(w_cgate, "fs", 0))
    conv_input = cgate * inner
    earlier = from_behind(conv_input[local_rows - (TAPS - 1) :], "fs", 1)
    padded = jnp.concatenate([earlier, conv_input], axis=0)
    conv = conv_taps[0] * padded[0:local_rows]
    for tap in range(1, TAPS):
        conv = conv + conv_taps[tap] * padded[tap : tap + local_rows]
    gated = (bgate * conv).astype(jnp.bfloat16)
    mix_partials = jnp.dot(gated, collect(w_out, "fs", 1), preferred_element_type=jnp.float32)
    second = settle(first, mix_partials, 3, 1.0)
    return feed_forward(second, 4, 5)


def solution(mesh):
    return jax.shard_map(
        shards,
        mesh=mesh,
        in_specs=(
            P(("rep", "fs"), "tp"),
            P(),
            P("fs", "tp"),
            P("fs", "tp"),
            P("tp", "fs"),
            P("fs", "tp"),
            P("fs", "tp"),
            P("fs", "tp"),
            P(None, "tp"),
            P("tp", "fs"),
        ),
        out_specs=P(("rep", "fs"), "tp"),
        check_vma=False,
    )
```

profile of v0, /device:TPU:1, one launch (start us, length us, event | category | flops | bytes accessed | tf_op | source)
XLA Modules:
  0.0 521.1 jit_solution(112186578533772279)
XLA Ops:
  9.5 24.3 %all_to_all.68 = bf16[8,256,256]{1,2,0:T(8,128)(2,1)S(1)} all-to-all(bf16[8,256,256]{1,2,0:T(8,128)(2,1)S(1)} %broadcast_in_dim.39), channel_id=1, replica_groups=mesh['rep'=2,'fs'=32,'tp'=8] {'tp'}, dimensions={0} | all-to-all | bytes 2097152 | tf_op jit(solution)/shard_map/all_to_all | solution.py:18
  34.8 11.8 %all-to-all-start.5 = ((bf16[32,64,128]{2,1,0:T(8,128)(2,1)}), bf16[32,64,128]{2,1,0:T(8,128)(2,1)S(1)}, u32[]{:S(2)}, u32[]{:S(2)}) async-start(bf16[32,64,128]{2,1,0:T(8,128)(2,1)} %broadcast_in_dim.43), calls=%async_computation.5 | async-start | bytes 1048576 | tf_op jit(solution)/shard_map/all_to_all | solution.py:18
  48.0 186.2 %all-gather.2.cloned.1.call-done = bf16[2048,2112]{1,0:T(8,128)(2,1)} async-done(((bf16[64,2112]{1,0:T(8,128)(2,1)}), bf16[2048,2112]{1,0:T(8,128)(2,1)}) %all-gather.2.cloned.1.call-update) | async-done | bytes 8650768 | tf_op jit(solution)/shard_map/all_gather | solution.py:45
  234.2 3.2 fusion.10
  237.4 7.4 %fusion.12 = bf16[256,2048]{1,0:T(8,128)(2,1)S(1)} fusion(bf16[2048,2112]{1,0:T(8,128)(2,1)} %all-gather.2.cloned.1.call-done, bf16[256,2048]{0,1:T(8,128)(2,1)S(1)} %fusion.24, f32[256,704]{0,1:T(8,128)S(1)} %fusion.10), kind=kOutput, calls=%fused_computation.15 | convolution fusion | flops 1478000640 | bytes 9109504 | tf_op jit(solution)/shard_map/dot_general | solution.py:88
  245.8 41.3 %all_to_all.69 = bf16[8,256,256]{2,1,0:T(8,128)(2,1)S(1)} all-to-all(bf16[8,256,256]{2,1,0:T(8,128)(2,1)S(1)} %bitcast.73), channel_id=1, replica_groups=mesh['rep'=2,'fs'=32,'tp'=8] {'tp'}, dimensions={0} | all-to-all | bytes 2097152 | tf_op jit(solution)/shard_map/all_to_all | solution.py:33
  288.0 8.5 %all-to-all-start.6 = ((bf16[32,64,128]{2,1,0:T(8,128)(2,1)}), bf16[32,64,128]{2,1,0:T(8,128)(2,1)S(1)}, u32[]{:S(2)}, u32[]{:S(2)}) async-start(bf16[32,64,128]{2,1,0:T(8,128)(2,1)} %broadcast_in_dim.44), calls=%async_computation.6 | async-start | bytes 1048576 | tf_op jit(solution)/shard_map/all_to_all | solution.py:18
  296.8 26.5 %all-to-all-done.6 = bf16[32,64,128]{2,1,0:T(8,128)(2,1)S(1)} async-done(((bf16[32,64,128]{2,1,0:T(8,128)(2,1)}), bf16[32,64,128]{2,1,0:T(8,128)(2,1)S(1)}, u32[]{:S(2)}, u32[]{:S(2)}) %all-to-all-start.6) | async-done | bytes 524320 | tf_op jit(solution)/shard_map/all_to_all | solution.py:18
  323.3 10.8 %all_to_all.70 = f32[8,1,256]{2,1,0:T(1,128)S(1)} all-to-all(f32[8,1,256]{2,1,0:T(1,128)S(1)} %broadcast_in_dim.40), channel_id=1, replica_groups=mesh['rep'=2,'fs'=32,'tp'=8] {'tp'}, dimensions={0} | all-to-all | bytes 16384 | tf_op jit(solution)/shard_map/all_to_all | solution.py:18
  335.0 5.8 %all-to-all-start.7 = ((bf16[32,128,64]{1,2,0:T(8,128)(2,1)}), bf16[32,128,64]{1,2,0:T(8,128)(2,1)S(1)}, u32[]{:S(2)}, u32[]{:S(2)}) async-start(bf16[32,128,64]{1,2,0:T(8,128)(2,1)} %broadcast_in_dim.45), calls=%async_computation.7 | async-start | bytes 1048576 | tf_op jit(solution)/shard_map/all_to_all | solution.py:18
  341.7 25.8 %all-to-all-done.7 = bf16[32,128,64]{1,2,0:T(8,128)(2,1)S(1)} async-done(((bf16[32,128,64]{1,2,0:T(8,128)(2,1)}), bf16[32,128,64]{1,2,0:T(8,128)(2,1)S(1)}, u32[]{:S(2)}, u32[]{:S(2)}) %all-to-all-start.7) | async-done | bytes 524320 | tf_op jit(solution)/shard_map/all_to_all | solution.py:18
  367.6 21.2 %all_to_all.71 = bf16[8,256,256]{1,2,0:T(8,128)(2,1)S(1)} all-to-all(bf16[8,256,256]{1,2,0:T(8,128)(2,1)S(1)} %broadcast_in_dim.41), channel_id=1, replica_groups=mesh['rep'=2,'fs'=32,'tp'=8] {'tp'}, dimensions={0} | all-to-all | bytes 2097152 | tf_op jit(solution)/shard_map/all_to_all | solution.py:18
  389.7 5.9 %all-to-all-start.4 = ((bf16[32,64,128]{2,1,0:T(8,128)(2,1)}), bf16[32,64,128]{2,1,0:T(8,128)(2,1)}, u32[]{:S(2)}, u32[]{:S(2)}) async-start(bf16[32,64,128]{2,1,0:T(8,128)(2,1)} %broadcast_in_dim.42), calls=%async_computation.4 | async-start | bytes 1048576 | tf_op jit(solution)/shard_map/all_to_all | solution.py:18
  398.4 3.1 collective-permute-start
  401.5 20.9 %all-to-all-done.4 = bf16[32,64,128]{2,1,0:T(8,128)(2,1)} async-done(((bf16[32,64,128]{2,1,0:T(8,128)(2,1)}), bf16[32,64,128]{2,1,0:T(8,128)(2,1)}, u32[]{:S(2)}, u32[]{:S(2)}) %all-to-all-start.4) | async-done | bytes 524320 | tf_op jit(solution)/shard_map/all_to_all | solution.py:18
  424.4 21.4 %all_to_all.72 = bf16[8,256,256]{2,1,0:T(8,128)(2,1)S(1)} all-to-all(bf16[8,256,256]{2,1,0:T(8,128)(2,1)S(1)} %bitcast.74), channel_id=1, replica_groups=mesh['rep'=2,'fs'=32,'tp'=8] {'tp'}, dimensions={0} | all-to-all | bytes 2097152 | tf_op jit(solution)/shard_map/all_to_all | solution.py:33
  446.6 4.3 all-to-all-start.9
  451.5 4.0 all-to-all-done.9
  455.8 18.1 %all_to_all.73 = bf16[8,256,256]{1,2,0:T(8,128)(2,1)S(1)} all-to-all(bf16[8,256,256]{1,2,0:T(8,128)(2,1)S(1)} %broadcast_in_dim.47), channel_id=1, replica_groups=mesh['rep'=2,'fs'=32,'tp'=8] {'tp'}, dimensions={0} | all-to-all | bytes 2097152 | tf_op jit(solution)/shard_map/all_to_all | solution.py:18
  474.5 3.2 fusion.8
  477.7 7.4 %fusion.15 = bf16[256,2048]{1,0:T(8,128)(2,1)S(1)} fusion(bf16[2048,2112]{1,0:T(8,128)(2,1)} %all-gather.2.cloned.1.call-done, bf16[256,2048]{0,1:T(8,128)(2,1)S(1)} %fusion.22, f32[256,704]{0,1:T(8,128)S(1)} %fusion.8), kind=kOutput, calls=%fused_computation.16 | convolution fusion | flops 1478000640 | bytes 9109504 | tf_op jit(solution)/shard_map/dot_general | solution.py:88
  485.2 18.4 %all_to_all.74 = bf16[8,256,256]{2,1,0:T(8,128)(2,1)S(1)} all-to-all(bf16[8,256,256]{2,1,0:T(8,128)(2,1)S(1)} %bitcast.75), channel_id=1, replica_groups=mesh['rep'=2,'fs'=32,'tp'=8] {'tp'}, dimensions={0} | all-to-all | bytes 2097152 | tf_op jit(solution)/shard_map/all_to_all | solution.py:33
  504.5 4.3 all-to-all-start.12
  509.4 4.0 all-to-all-done.12
  (71 shorter events, 19.6 us)
Async XLA Ops:
  6.5 227.7 %all-gather.2.cloned.1.call-start = ((), (), s32[]{:S(2)}) async-start(), calls=%async_computation.13 | async-start | bytes 9191424 | tf_op jit(solution)/shard_map/all_gather | solution.py:45
  6.5 27.3 %copy-start.3 = (bf16[64,128]{1,0:T(8,128)(2,1)S(1)}, bf16[64,128]{1,0:T(8,128)(2,1)}, u32[]{:S(2)}) copy-start(bf16[64,128]{1,0:T(8,128)(2,1)} %param.17) | copy-start | bytes 49156
  9.5 37.2 %copy-start.2 = (f32[6,2048]{1,0:T(8,128)S(1)}, f32[6,2048]{1,0:T(8,128)}, u32[]{:S(2)}) copy-start(f32[6,2048]{1,0:T(8,128)} %param.11) | copy-start | bytes 147460
  34.8 210.1 %all-to-all-start.5 = ((bf16[32,64,128]{2,1,0:T(8,128)(2,1)}), bf16[32,64,128]{2,1,0:T(8,128)(2,1)S(1)}, u32[]{:S(2)}, u32[]{:S(2)}) async-start(bf16[32,64,128]{2,1,0:T(8,128)(2,1)} %broadcast_in_dim.43), calls=%async_computation.5 | async-start | bytes 1048576 | tf_op jit(solution)/shard_map/all_to_all | solution.py:18
  244.9 42.2 %copy-start.4 = (bf16[64,128]{1,0:T(8,128)(2,1)S(1)}, bf16[64,128]{1,0:T(8,128)(2,1)}, u32[]{:S(2)}) copy-start(bf16[64,128]{1,0:T(8,128)(2,1)} %param.15) | copy-start | bytes 49156
  244.9 0.9 copy-start
  287.1 47.0 %copy-start.5 = (bf16[128,64]{0,1:T(8,128)(2,1)S(1)}, bf16[128,64]{0,1:T(8,128)(2,1)}, u32[]{:S(2)}) copy-start(bf16[128,64]{0,1:T(8,128)(2,1)} %param.19) | copy-start | bytes 49156
  288.0 53.5 %copy-start.1 = (bf16[256,256]{1,0:T(8,128)(2,1)S(1)}, bf16[256,256]{1,0:T(8,128)(2,1)}, u32[]{:S(2)}) copy-start(bf16[256,256]{1,0:T(8,128)(2,1)} %param.10) | copy-start | bytes 393220
  288.0 35.3 %all-to-all-start.6 = ((bf16[32,64,128]{2,1,0:T(8,128)(2,1)}), bf16[32,64,128]{2,1,0:T(8,128)(2,1)S(1)}, u32[]{:S(2)}, u32[]{:S(2)}) async-start(bf16[32,64,128]{2,1,0:T(8,128)(2,1)} %broadcast_in_dim.44), calls=%async_computation.6 | async-start | bytes 1048576 | tf_op jit(solution)/shard_map/all_to_all | solution.py:18
  335.0 32.6 %all-to-all-start.7 = ((bf16[32,128,64]{1,2,0:T(8,128)(2,1)}), bf16[32,128,64]{1,2,0:T(8,128)(2,1)S(1)}, u32[]{:S(2)}, u32[]{:S(2)}) async-start(bf16[32,128,64]{1,2,0:T(8,128)(2,1)} %broadcast_in_dim.45), calls=%async_computation.7 | async-start | bytes 1048576 | tf_op jit(solution)/shard_map/all_to_all | solution.py:18
  340.8 48.0 %copy-start.6 = (bf16[64,128]{1,0:T(8,128)(2,1)S(1)}, bf16[64,128]{1,0:T(8,128)(2,1)}, u32[]{:S(2)}) copy-start(bf16[64,128]{1,0:T(8,128)(2,1)} %param.16) | copy-start | bytes 49156
  389.7 32.7 %all-to-all-start.4 = ((bf16[32,64,128]{2,1,0:T(8,128)(2,1)}), bf16[32,64,128]{2,1,0:T(8,128)(2,1)}, u32[]{:S(2)}, u32[]{:S(2)}) async-start(bf16[32,64,128]{2,1,0:T(8,128)(2,1)} %broadcast_in_dim.42), calls=%async_computation.4 | async-start | bytes 1048576 | tf_op jit(solution)/shard_map/all_to_all | solution.py:18
  396.4 5.1 copy-start.7
  398.4 24.0 %collective-permute-start = (f32[2,128]{1,0:T(2,128)S(1)}, f32[2,128]{1,0:T(2,128)S(1)}, u32[]{:S(2)}, u32[]{:S(2)}) collective-permute-start(f32[2,128]{1,0:T(2,128)S(1)} %slice.63), channel_id=1, source_target_pairs={{0,8},{8,16},{16,24},{24,32},{32,40},{40,48},{48,56},{56,64},{64,7... | collective-permute-start | bytes 3080 | tf_op jit(solution)/shard_map/ppermute | solution.py:56
  446.6 8.9 %all-to-all-start.9 = ((f32[8,1,256]{2,1,0:T(1,128)}), f32[8,1,256]{2,1,0:T(1,128)S(1)}, u32[]{:S(2)}, u32[]{:S(2)}) async-start(f32[8,1,256]{2,1,0:T(1,128)} %broadcast_in_dim.46), calls=%async_computation.9 | async-start | bytes 16384 | tf_op jit(solution)/shard_map/all_to_all | solution.py:18
  504.5 8.9 %all-to-all-start.12 = ((f32[8,1,256]{2,1,0:T(1,128)}), f32[8,1,256]{2,1,0:T(1,128)S(1)}, u32[]{:S(2)}, u32[]{:S(2)}) async-start(f32[8,1,256]{2,1,0:T(1,128)} %broadcast_in_dim.48), calls=%async_computation.12 | async-start | bytes 16384 | tf_op jit(solution)/shard_map/all_to_all | solution.py:18
Sparse Core Ops, SparseCore 0:
  9.4 224.7 all-gather.1
where the time goes:
time: 522 us; the launch traced here: 521 us
  waiting for transfers between devices  267 us (51%)
  blocking collectives  155 us (30%)
  starting transfers between devices  43.7 us (8%)
  matrix products  25 us (5%)
  between operations  13.7 us (3%)
  local copies, waits for them, and re-layouts  11.8 us (2%)
    all_gather x1, waiting for transfers between devices, rows_first(): whole, at, done = (lax.all_gather(both, axis, axis=0, tiled=True), 0, [])  186 us
    all_to_all x6, waiting for transfers between devices, from_everyone(): return lax.all_to_all(copies, axis, split_axis=0, concat_axis=0, tiled=True)  81.2 us
    all_to_all x3, blocking collectives, sent_and_summed(): lax.all_to_all(parts, axis, split_axis=0, concat_axis=0, tiled=True)  81.1 us
    all_to_all x4, blocking collectives, from_everyone(): return lax.all_to_all(copies, axis, split_axis=0, concat_axis=0, tiled=True)  74.4 us
    all_to_all x6, starting transfers between devices, from_everyone(): return lax.all_to_all(copies, axis, split_axis=0, concat_axis=0, tiled=True)  40.6 us
    dot_general x2, matrix products, feed_forward(): partials = jnp.dot(hidden, down_whole, preferred_element_type=jnp.float32)  14.8 us
  transfers between devices with their start and end apart: 8, of which 6 were waited for; matrix products, arithmetic and copies ran while one was open for 4% of the time, Pallas kernels for 0%

commit v1 on v0

--- a/solution.py
+++ b/solution.py
@@ -42,7 +42,13 @@
 def rows_first(arrays, axis, dims):
     turned = [jnp.moveaxis(a, dim, 0) for a, dim in zip(arrays, dims)]
     both = jnp.concatenate([t.reshape(len(t), -1) for t in turned], axis=1)
-    whole, at, done = (lax.all_gather(both, axis, axis=0, tiled=True), 0, [])
+    whole, at, done = (
+        jnp.concatenate(
+            lax.all_to_all(jnp.stack([both] * lax.axis_size(axis)), axis, 0, 0), axis=0
+        ),
+        0,
+        [],
+    )
     for t, dim in zip(turned, dims):
         slab = whole[:, at : at + t[0].size].reshape(-1, *t.shape[1:])
         done.append(jnp.moveaxis(slab, 0, dim))

time: 522 us -> 709 us (1.36)
  blocking collectives: 155 us -> 510 us
  waiting for transfers between devices: 267 us -> 113 us
  between operations: 13.7 us -> 0.36 us
    all_to_all x0 -> x1, blocking collectives: none -> 399 us  [rows_first(): lax.all_to_all(jnp.stack([both] * lax.axis_size(axis)), axis, 0, 0)]
    all_gather x1 -> x0, waiting for transfers between devices: 186 us -> none  [rows_first(): whole, at, done = (lax.all_gather(both, axis, axis=0, tiled=True), 0, [])]
    all_to_all x6 -> x7, waiting for transfers between devices: 81.2 us -> 113 us  [from_everyone(): return lax.all_to_all(copies, axis, split_axis=0, concat_axis=0, tiled=True)]
    all_to_all x4 -> x3, blocking collectives: 74.4 us -> 50.1 us  [from_everyone(): return lax.all_to_all(copies, axis, split_axis=0, concat_axis=0, tiled=True)]
    all_to_all x3, blocking collectives: 81.1 us -> 60.8 us  [sent_and_summed(): lax.all_to_all(parts, axis, split_axis=0, concat_axis=0, tiled=True)]
    all_to_all x6 -> x7, starting transfers between devices: 40.6 us -> 43.7 us  [from_everyone(): return lax.all_to_all(copies, axis, split_axis=0, concat_axis=0, tiled=True)]
  transfers between devices with their start and end apart: 8 -> 8, of which waited for: 6 -> 7; matrix products, arithmetic and copies ran while one was open for 4% -> 2% of each run, Pallas kernels for 0% -> 0%
where the time goes in v1:
time: 709 us; the launch traced here: 708 us
  blocking collectives  510 us (72%)
  waiting for transfers between devices  113 us (16%)
  starting transfers between devices  46.6 us (7%)
  matrix products  25 us (4%)
  local copies, waits for them, and re-layouts  9.1 us (1%)
    all_to_all x1, blocking collectives, rows_first(): lax.all_to_all(jnp.stack([both] * lax.axis_size(axis)), axis, 0, 0)  399 us
    all_to_all x7, waiting for transfers between devices, from_everyone(): return lax.all_to_all(copies, axis, split_axis=0, concat_axis=0, tiled=True)  113 us
    all_to_all x3, blocking collectives, sent_and_summed(): lax.all_to_all(parts, axis, split_axis=0, concat_axis=0, tiled=True)  60.8 us
    all_to_all x3, blocking collectives, from_everyone(): return lax.all_to_all(copies, axis, split_axis=0, concat_axis=0, tiled=True)  50.1 us
    all_to_all x7, starting transfers between devices, from_everyone(): return lax.all_to_all(copies, axis, split_axis=0, concat_axis=0, tiled=True)  43.7 us
    dot_general x2, matrix products, feed_forward(): partials = jnp.dot(hidden, down_whole, preferred_element_type=jnp.float32)  14.8 us
  transfers between devices with their start and end apart: 8, of which 7 were waited for; matrix products, arithmetic and copies ran while one was open for 2% of the time, Pallas kernels for 0%

profile of v1, /device:TPU:1, one launch (start us, length us, event | category | flops | bytes accessed | tf_op | source)
XLA Modules:
  0.0 708.0 jit_solution(3756277491699097522)
XLA Ops:
  2.1 10.3 %all-to-all-start = ((bf16[8,256,256]{1,2,0:T(8,128)(2,1)}), bf16[8,256,256]{1,2,0:T(8,128)(2,1)S(1)}, u32[]{:S(2)}, u32[]{:S(2)}) async-start(bf16[8,256,256]{1,2,0:T(8,128)(2,1)} %broadcast_in_dim.39), calls=%async_computation | async-start | bytes 2097152 | tf_op jit(solution)/shard_map/all_to_all | solution.py:18
  12.6 14.8 %all-to-all-done = bf16[8,256,256]{1,2,0:T(8,128)(2,1)S(1)} async-done(((bf16[8,256,256]{1,2,0:T(8,128)(2,1)}), bf16[8,256,256]{1,2,0:T(8,128)(2,1)S(1)}, u32[]{:S(2)}, u32[]{:S(2)}) %all-to-all-start) | async-done | bytes 1048608 | tf_op jit(solution)/shard_map/all_to_all | solution.py:18
  28.6 399.0 %all_to_all.73 = bf16[32,64,2112]{2,1,0:T(8,128)(2,1)} all-to-all(bf16[32,64,2112]{2,1,0:T(8,128)(2,1)S(1)} %stack.2), channel_id=1, replica_groups=mesh['rep'=2,'fs'=32,'tp'=8] {'fs'}, dimensions={0} | all-to-all | bytes 17301504 | tf_op jit(solution)/shard_map/all_to_all | solution.py:47
  428.6 7.0 all-to-all-start.8
  439.5 7.4 %fusion.12 = bf16[256,2048]{1,0:T(8,128)(2,1)S(1)} fusion(bf16[2048,2112]{1,0:T(8,128)(2,1)} %bitcast.74, bf16[256,2048]{0,1:T(8,128)(2,1)S(1)} %fusion.24, f32[256,704]{0,1:T(8,128)S(1)} %fusion.10), kind=kOutput, calls=%fused_computation.15 | convolution fusion | flops 1478000640 | bytes 9109504 | tf_op jit(solution)/shard_map/dot_general | solution.py:94
  447.0 15.3 %all-to-all-done.8 = bf16[32,128,64]{1,2,0:T(8,128)(2,1)S(1)} async-done(((bf16[32,128,64]{1,2,0:T(8,128)(2,1)}), bf16[32,128,64]{1,2,0:T(8,128)(2,1)S(1)}, u32[]{:S(2)}, u32[]{:S(2)}) %all-to-all-start.8) | async-done | bytes 524320 | tf_op jit(solution)/shard_map/all_to_all | solution.py:18
  462.4 21.2 %all_to_all.74 = bf16[8,256,256]{2,1,0:T(8,128)(2,1)S(1)} all-to-all(bf16[8,256,256]{2,1,0:T(8,128)(2,1)S(1)} %bitcast.78), channel_id=1, replica_groups=mesh['rep'=2,'fs'=32,'tp'=8] {'tp'}, dimensions={0} | all-to-all | bytes 2097152 | tf_op jit(solution)/shard_map/all_to_all | solution.py:33
  484.5 5.9 all-to-all-start.6
  490.7 26.5 %all-to-all-done.6 = bf16[32,64,128]{2,1,0:T(8,128)(2,1)S(1)} async-done(((bf16[32,64,128]{2,1,0:T(8,128)(2,1)}), bf16[32,64,128]{2,1,0:T(8,128)(2,1)S(1)}, u32[]{:S(2)}, u32[]{:S(2)}) %all-to-all-start.6) | async-done | bytes 524320 | tf_op jit(solution)/shard_map/all_to_all | solution.py:18
  517.2 10.8 %all_to_all.75 = f32[8,1,256]{2,1,0:T(1,128)S(1)} all-to-all(f32[8,1,256]{2,1,0:T(1,128)S(1)} %broadcast_in_dim.40), channel_id=1, replica_groups=mesh['rep'=2,'fs'=32,'tp'=8] {'tp'}, dimensions={0} | all-to-all | bytes 16384 | tf_op jit(solution)/shard_map/all_to_all | solution.py:18
  529.0 5.8 all-to-all-start.7
  535.1 26.4 %all-to-all-done.7 = bf16[32,64,128]{2,1,0:T(8,128)(2,1)S(1)} async-done(((bf16[32,64,128]{2,1,0:T(8,128)(2,1)}), bf16[32,64,128]{2,1,0:T(8,128)(2,1)S(1)}, u32[]{:S(2)}, u32[]{:S(2)}) %all-to-all-start.7) | async-done | bytes 524320 | tf_op jit(solution)/shard_map/all_to_all | solution.py:18
  561.6 21.2 %all_to_all.76 = bf16[8,256,256]{1,2,0:T(8,128)(2,1)S(1)} all-to-all(bf16[8,256,256]{1,2,0:T(8,128)(2,1)S(1)} %broadcast_in_dim.41), channel_id=1, replica_groups=mesh['rep'=2,'fs'=32,'tp'=8] {'tp'}, dimensions={0} | all-to-all | bytes 2097152 | tf_op jit(solution)/shard_map/all_to_all | solution.py:18
  583.7 6.1 all-to-all-start.5
  595.5 20.9 %all-to-all-done.5 = bf16[32,64,128]{2,1,0:T(8,128)(2,1)} async-done(((bf16[32,64,128]{2,1,0:T(8,128)(2,1)}), bf16[32,64,128]{2,1,0:T(8,128)(2,1)}, u32[]{:S(2)}, u32[]{:S(2)}) %all-to-all-start.5) | async-done | bytes 524320 | tf_op jit(solution)/shard_map/all_to_all | solution.py:18
  618.3 21.2 %all_to_all.77 = bf16[8,256,256]{2,1,0:T(8,128)(2,1)S(1)} all-to-all(bf16[8,256,256]{2,1,0:T(8,128)(2,1)S(1)} %bitcast.79), channel_id=1, replica_groups=mesh['rep'=2,'fs'=32,'tp'=8] {'tp'}, dimensions={0} | all-to-all | bytes 2097152 | tf_op jit(solution)/shard_map/all_to_all | solution.py:33
  640.4 4.3 all-to-all-start.10
  644.7 4.6 all-to-all-done.10
  649.6 18.1 %all_to_all.78 = bf16[8,256,256]{1,2,0:T(8,128)(2,1)S(1)} all-to-all(bf16[8,256,256]{1,2,0:T(8,128)(2,1)S(1)} %broadcast_in_dim.47), channel_id=1, replica_groups=mesh['rep'=2,'fs'=32,'tp'=8] {'tp'}, dimensions={0} | all-to-all | bytes 2097152 | tf_op jit(solution)/shard_map/all_to_all | solution.py:18
  668.4 3.2 fusion.8
  671.6 7.4 %fusion.15 = bf16[256,2048]{1,0:T(8,128)(2,1)S(1)} fusion(bf16[2048,2112]{1,0:T(8,128)(2,1)} %bitcast.76, bf16[256,2048]{0,1:T(8,128)(2,1)S(1)} %fusion.22, f32[256,704]{0,1:T(8,128)S(1)} %fusion.8), kind=kOutput, calls=%fused_computation.16 | convolution fusion | flops 1478000640 | bytes 9109504 | tf_op jit(solution)/shard_map/dot_general | solution.py:94
  679.0 18.4 %all_to_all.79 = bf16[8,256,256]{2,1,0:T(8,128)(2,1)S(1)} all-to-all(bf16[8,256,256]{2,1,0:T(8,128)(2,1)S(1)} %bitcast.80), channel_id=1, replica_groups=mesh['rep'=2,'fs'=32,'tp'=8] {'tp'}, dimensions={0} | all-to-all | bytes 2097152 | tf_op jit(solution)/shard_map/all_to_all | solution.py:33
  698.3 4.3 all-to-all-start.13
  702.6 4.6 all-to-all-done.13
  (77 shorter events, 22.9 us)
Async XLA Ops:
  0.0 12.4 %copy-start.2 = (bf16[64,704]{1,0:T(8,128)(2,1)S(1)}, bf16[64,704]{1,0:T(8,128)(2,1)}, u32[]{:S(2)}) copy-start(bf16[64,704]{1,0:T(8,128)(2,1)} %param.12) | copy-start | bytes 270340
  0.0 12.4 %copy-start.3 = (bf16[64,704]{1,0:T(8,128)(2,1)S(1)}, bf16[64,704]{1,0:T(8,128)(2,1)}, u32[]{:S(2)}) copy-start(bf16[64,704]{1,0:T(8,128)(2,1)} %param.13) | copy-start | bytes 270340
  0.0 12.4 %copy-start.4 = (bf16[704,64]{0,1:T(8,128)(2,1)S(1)}, bf16[704,64]{0,1:T(8,128)(2,1)}, u32[]{:S(2)}) copy-start(bf16[704,64]{0,1:T(8,128)(2,1)} %param.14) | copy-start | bytes 270340
  2.1 25.3 %all-to-all-start = ((bf16[8,256,256]{1,2,0:T(8,128)(2,1)}), bf16[8,256,256]{1,2,0:T(8,128)(2,1)S(1)}, u32[]{:S(2)}, u32[]{:S(2)}) async-start(bf16[8,256,256]{1,2,0:T(8,128)(2,1)} %broadcast_in_dim.39), calls=%async_computation | async-start | bytes 2097152 | tf_op jit(solution)/shard_map/all_to_all | solution.py:18
  28.6 399.0 %copy-start.6 = (bf16[128,64]{0,1:T(8,128)(2,1)S(1)}, bf16[128,64]{0,1:T(8,128)(2,1)}, u32[]{:S(2)}) copy-start(bf16[128,64]{0,1:T(8,128)(2,1)} %param.19) | copy-start | bytes 49156
  28.6 407.0 %copy-start.5 = (f32[6,2048]{1,0:T(8,128)S(1)}, f32[6,2048]{1,0:T(8,128)}, u32[]{:S(2)}) copy-start(f32[6,2048]{1,0:T(8,128)} %param.11) | copy-start | bytes 147460
  428.6 33.7 %all-to-all-start.8 = ((bf16[32,128,64]{1,2,0:T(8,128)(2,1)}), bf16[32,128,64]{1,2,0:T(8,128)(2,1)S(1)}, u32[]{:S(2)}, u32[]{:S(2)}) async-start(bf16[32,128,64]{1,2,0:T(8,128)(2,1)} %broadcast_in_dim.45), calls=%async_computation.8 | async-start | bytes 1048576 | tf_op jit(solution)/shard_map/all_to_all | solution.py:18
  446.9 36.6 %copy-start.7 = (bf16[64,128]{1,0:T(8,128)(2,1)S(1)}, bf16[64,128]{1,0:T(8,128)(2,1)}, u32[]{:S(2)}) copy-start(bf16[64,128]{1,0:T(8,128)(2,1)} %param.17) | copy-start | bytes 49156
  483.5 44.5 %copy-start.8 = (bf16[64,128]{1,0:T(8,128)(2,1)S(1)}, bf16[64,128]{1,0:T(8,128)(2,1)}, u32[]{:S(2)}) copy-start(bf16[64,128]{1,0:T(8,128)(2,1)} %param.15) | copy-start | bytes 49156
  484.5 50.3 %copy-start.1 = (bf16[256,256]{1,0:T(8,128)(2,1)S(1)}, bf16[256,256]{1,0:T(8,128)(2,1)}, u32[]{:S(2)}) copy-start(bf16[256,256]{1,0:T(8,128)(2,1)} %param.10) | copy-start | bytes 393220
  484.5 32.7 %all-to-all-start.6 = ((bf16[32,64,128]{2,1,0:T(8,128)(2,1)}), bf16[32,64,128]{2,1,0:T(8,128)(2,1)S(1)}, u32[]{:S(2)}, u32[]{:S(2)}) async-start(bf16[32,64,128]{2,1,0:T(8,128)(2,1)} %broadcast_in_dim.43), calls=%async_computation.6 | async-start | bytes 1048576 | tf_op jit(solution)/shard_map/all_to_all | solution.py:18
  517.2 11.7 %copy-start = (bf16[32,64,128]{2,1,0:T(8,128)(2,1)}, bf16[32,64,128]{2,1,0:T(8,128)(2,1)S(1)}, u32[]{:S(2)}) copy-start(bf16[32,64,128]{2,1,0:T(8,128)(2,1)S(1)} %all-to-all-done.6) | copy-start | bytes 1572868
  529.0 32.6 %all-to-all-start.7 = ((bf16[32,64,128]{2,1,0:T(8,128)(2,1)}), bf16[32,64,128]{2,1,0:T(8,128)(2,1)S(1)}, u32[]{:S(2)}, u32[]{:S(2)}) async-start(bf16[32,64,128]{2,1,0:T(8,128)(2,1)} %broadcast_in_dim.44), calls=%async_computation.7 | async-start | bytes 1048576 | tf_op jit(solution)/shard_map/all_to_all | solution.py:18
  534.8 48.0 %copy-start.9 = (bf16[64,128]{1,0:T(8,128)(2,1)S(1)}, bf16[64,128]{1,0:T(8,128)(2,1)}, u32[]{:S(2)}) copy-start(bf16[64,128]{1,0:T(8,128)(2,1)} %param.16) | copy-start | bytes 49156
  583.7 32.7 %all-to-all-start.5 = ((bf16[32,64,128]{2,1,0:T(8,128)(2,1)}), bf16[32,64,128]{2,1,0:T(8,128)(2,1)}, u32[]{:S(2)}, u32[]{:S(2)}) async-start(bf16[32,64,128]{2,1,0:T(8,128)(2,1)} %broadcast_in_dim.42), calls=%async_computation.5 | async-start | bytes 1048576 | tf_op jit(solution)/shard_map/all_to_all | solution.py:18
  590.5 4.9 copy-start.10
  592.5 23.8 %collective-permute-start = (f32[2,128]{1,0:T(2,128)S(1)}, f32[2,128]{1,0:T(2,128)S(1)}, u32[]{:S(2)}, u32[]{:S(2)}) collective-permute-start(f32[2,128]{1,0:T(2,128)S(1)} %slice.63), channel_id=1, source_target_pairs={{0,8},{8,16},{16,24},{24,32},{32,40},{40,48},{48,56},{56,64},{64,7... | collective-permute-start | bytes 3080 | tf_op jit(solution)/shard_map/ppermute | solution.py:62
  640.4 8.9 %all-to-all-start.10 = ((f32[8,1,256]{2,1,0:T(1,128)}), f32[8,1,256]{2,1,0:T(1,128)S(1)}, u32[]{:S(2)}, u32[]{:S(2)}) async-start(f32[8,1,256]{2,1,0:T(1,128)} %broadcast_in_dim.46), calls=%async_computation.10 | async-start | bytes 16384 | tf_op jit(solution)/shard_map/all_to_all | solution.py:18
  698.3 8.9 %all-to-all-start.13 = ((f32[8,1,256]{2,1,0:T(1,128)}), f32[8,1,256]{2,1,0:T(1,128)S(1)}, u32[]{:S(2)}, u32[]{:S(2)}) async-start(f32[8,1,256]{2,1,0:T(1,128)} %broadcast_in_dim.48), calls=%async_computation.13 | async-start | bytes 16384 | tf_op jit(solution)/shard_map/all_to_all | solution.py:18
